TPU v7x, 512 devices: a 8x2x16 block of a 8x8x16 slice. The times are simulated.
512 devices in a mesh: grp: 2 (over y), sp: 16 (over z), dp: 16 (over x, core).
Axes of the slice: x: 8, y: 2, z: 16, core: 2. Of those that a mesh axis runs over, the one named last changes fastest.
The devices are a block of a 8x8x16 slice.
Arguments:
- queries: bfloat16 [32, 2048, 16, 192], P(('grp', 'dp'), 'sp'), parts along dimension 0, may hold values from -41 to 41
- kv_latent: bfloat16 [32, 2048, 512], P(('grp', 'dp'), 'sp'), parts along dimension 0, may hold values from -6 to 6
- rope_key: bfloat16 [32, 2048, 64], P(('grp', 'dp'), 'sp'), parts along dimension 0, may hold values from -5.1 to 5.1
- kv_gain: float32 [512], replicated, may hold values from 0.1 to 1.9
- kv_weight: bfloat16 [512, 4096], P('dp', 'sp'), may hold values from -0.25 to 0.25
- out_weight: bfloat16 [2048, 2048], P(None, 'dp'), may hold values from -1 to 1
Outputs:
- mixed: bfloat16 [32, 2048, 2048], P(('grp', 'dp'), 'sp'), parts along dimension 0
There are 2 independent parts, one for each index of `grp`. A program takes and returns all parts, laid end to end along the dimension named above; an argument that names none is the same for every part. Nothing has to cross between parts.
All inputs are finite; a program needn't handle non-finite values.
Results may differ from a plain program's by a relative error of at most 0.0075.
Values may be sent and summed in bfloat16 or wider, within the bound.
A program may use at most 64 MiB of HBM per device.

v0:
```python
import jax
import jax.numpy as jnp
from jax import lax
from jax.sharding import PartitionSpec as P

NOPE = 128
VD = 128


def sent_to_all(value, axis):
    length = lax.axis_size(axis)
    return lax.all_to_all(
        jnp.broadcast_to(value[None], (length, *value.shape)), axis, 0, 0, tiled=True
    )


def in_order(parts, dim):
    parts = jnp.moveaxis(parts, 0, dim)
    dims = parts.shape
    return parts.reshape(*dims[:dim], dims[dim] * dims[dim + 1], *dims[dim + 2 :])


def gather_directly(value, axis, dim):
    parts = sent_to_all(value, axis)
    return in_order(parts, dim)


def rotate(values, positions):
    half = values.shape[-1] // 2
    inverse = jnp.power(10000.0, -jnp.arange(half, dtype=jnp.float32) * 2.0 / values.shape[-1])
    angle = positions.astype(jnp.float32)[..., None] * inverse
    first = values[..., :half].astype(jnp.float32)
    second = values[..., half:].astype(jnp.float32)
    cosine = jnp.cos(angle)
    sine = jnp.sin(angle)
    return jnp.concatenate(
        [first * cosine - second * sine, first * sine + second * cosine], axis=-1
    )


def attend(query_rot, key_value, key_rot):
    length, heads = (query_rot.shape[0], query_rot.shape[1])
    nope = query_rot.shape[2] - key_rot.shape[1]
    scale = query_rot.shape[2] ** (-0.5)
    content = key_value[:, :, :nope]
    values = key_value[:, :, nope:]
    shared = key_rot[:, None, :]
    keys = jnp.concatenate([content, shared], axis=-1)
    block = min(512, length)
    blocks = query_rot.reshape(length // block, block, heads, query_rot.shape[2])
    key_pos = jnp.arange(length, dtype=jnp.int32)

    def one_block(item):
        query_block, index = item
        scores = (
            jnp.einsum("qhd,khd->hqk", query_block, keys, preferred_element_type=jnp.float32)
            * scale
        )
        query_pos = index * block + jnp.arange(block, dtype=jnp.int32)
        kept = query_pos[:, None] >= key_pos[None, :]
        scores = jnp.where(kept[None], scores, -jnp.inf)
        top = jnp.max(scores, axis=-1, keepdims=True)
        expo = jnp.exp(scores - top)
        probs = (expo / jnp.sum(expo, axis=-1, keepdims=True)).astype(jnp.bfloat16)
        return jnp.einsum("hqk,khd->qhd", probs, values, preferred_element_type=jnp.float32).astype(
            jnp.bfloat16
        )

    result = lax.map(one_block, (blocks, jnp.arange(length // block, dtype=jnp.int32)))
    return result.reshape(length, heads, values.shape[2])


def body(queries, kv_latent, rope_key, kv_gain, kv_weight, out_weight):
    tok_rows = queries.shape[1]
    positions = lax.axis_index("sp") * tok_rows + jnp.arange(tok_rows, dtype=jnp.int32)
    latent32 = kv_latent[0].astype(jnp.float32)
    latent_n = (
        latent32
        * lax.rsqrt(jnp.mean(latent32 * latent32, axis=-1, keepdims=True) + 1e-06)
        * kv_gain
    ).astype(jnp.bfloat16)
    key_rot = rotate(rope_key[0], positions).astype(jnp.bfloat16)
    turned = rotate(queries[0, :, :, NOPE:], positions[:, None])
    query_rot = jnp.concatenate(
        [queries[0, :, :, :NOPE].astype(jnp.float32), turned], axis=-1
    ).astype(jnp.bfloat16)
    query_heads = lax.all_to_all(query_rot[None], "sp", split_axis=2, concat_axis=1, tiled=True)
    every_latent, every_key = (
        lax.all_gather(latent_n[None], "sp", axis=1, tiled=True),
        lax.all_gather(key_rot[None], "sp", axis=1, tiled=True),
    )
    whole_latent = every_latent[0]
    kv_heads = jnp.dot(
        whole_latent, gather_directly(kv_weight, "dp", 0), preferred_element_type=jnp.float32
    ).astype(jnp.bfloat16)
    kv_heads = kv_heads.reshape(whole_latent.shape[0], kv_weight.shape[1] // (NOPE + VD), NOPE + VD)
    attended = attend(query_heads[0], kv_heads, every_key[0])
    returned = lax.all_to_all(attended[None], "sp", split_axis=1, concat_axis=2, tiled=True)
    flat_rows = returned.reshape(tok_rows, returned.shape[2] * returned.shape[3])
    mixed = jnp.dot(
        flat_rows,
        lax.all_gather(out_weight, "dp", axis=1, tiled=True),
        preferred_element_type=jnp.float32,
    ).astype(jnp.bfloat16)
    return mixed[None]


def solution(mesh):
    return jax.shard_map(
        body,
        mesh=mesh,
        in_specs=(
            P(("grp", "dp"), "sp", None, None),
            P(("grp", "dp"), "sp", None),
            P(("grp", "dp"), "sp", None),
            P(),
            P("dp", "sp"),
            P(None, "dp"),
        ),
        out_specs=P(("grp", "dp"), "sp", None),
        check_vma=False,
    )
```

profile of v0, /device:TPU:84, one launch (start us, length us, event | category | flops | bytes accessed | tf_op | source)
XLA Modules:
  0.0 228.3 jit_solution(14194798245144524070)
XLA Ops:
  6.6 1.0 fusion.19
  7.6 1.7 fusion.21
  9.4 0.7 all-gather.5.cloned.1.call-update
  10.1 1.1 slice.32
  11.3 0.9 fusion.29
  12.1 1.0 slice_bitcast_fusion
  13.1 0.1 fusion.23
  13.3 91.7 %all_to_all.35 = bf16[1,128,16,192]{1,3,0,2:T(8,128)(2,1)S(1)} all-to-all(bf16[1,128,16,192]{1,3,0,2:T(8,128)(2,1)S(1)} %pad_maximum_fusion), channel_id=1, replica_groups=mesh['grp'=2,'sp'=16,'dp'=16] {'sp'}, dimensions={2} | all-to-all | bytes 1572864 | tf_op jit(solution)/shard_map/all_to_all | solution.py:87
  104.9 0.7 broadcast_in_dim.13
  105.7 7.8 %all-to-all-start.1 = ((bf16[16,32,256]{2,1,0:T(8,128)(2,1)}), bf16[16,32,256]{2,1,0:T(8,128)(2,1)S(1)}, u32[]{:S(2)}, u32[]{:S(2)}) async-start(bf16[16,32,256]{2,1,0:T(8,128)(2,1)} %broadcast_in_dim.13), calls=%async_computation.1 | async-start | bytes 524288 | tf_op jit(solution)/shard_map/all_to_all | solution.py:12
  113.5 32.2 %all_gather.10 = bf16[1,2048,64]{1,2,0:T(8,128)(2,1)S(1)} all-gather(bf16[1,128,64]{1,2,0:T(8,128)(2,1)S(1)} %pad_maximum_fusion.2), channel_id=1, replica_groups=mesh['grp'=2,'sp'=16,'dp'=16] {'sp'}, dimensions={1}, use_global_device_ids=true | all-gather | bytes 278528 | tf_op jit(solution)/shard_map/all_gather | solution.py:90
  145.7 0.5 copy.25
  146.2 0.3 reshape_squeeze.3
  146.5 0.1 copy.26
  146.7 2.3 %fusion.12 = bf16[2048,1,256]{0,2,1:T(8,128)(2,1)S(1)} fusion(bf16[512,256]{1,0:T(8,128)(2,1)S(1)} %bitcast.82, bf16[1,2048,512]{2,1,0:T(8,128)(2,1)} %all-gather.3.cloned.1.call-done), kind=kOutput, calls=%fused_computation.17 | convolution fusion | flops 537395200 | bytes 3407872 | tf_op jit(solution)/shard_map/dot_general | solution.py:93
  149.0 0.1 fusion.31
  149.1 1.0 copy.27
  150.1 0.1 pad_maximum_fusion.1
  150.2 16.9 %while.11 = (s32[]{:T(128)}, bf16[4,512,1,128]{3,1,2,0:T(8,128)(2,1)S(1)}, s32[4]{0:T(128)S(1)}, bf16[4,512,1,192]{1,3,2,0:T(8,128)(2,1)S(1)}, bf16[2048,1,192]{...) while((s32[]{:T(128)}, ...), condition=%wide.region_4.5_spmd.clone, body=%wide.region_1.4_spmd.clone.sunk | while | flops 680590848 | bytes 16332949 | solution.py:69
  150.4 0.6 dynamic_slice.19
  151.5 1.0 fusion.40
  152.5 0.7 fusion.41
  153.2 0.4 copy-done
  153.7 0.9 fusion.42
  154.6 0.6 dynamic_slice.19
  155.8 1.0 fusion.40
  156.8 0.7 fusion.41
  157.5 0.3 copy-done
  157.8 0.9 fusion.42
  158.8 0.6 dynamic_slice.19
  159.9 1.0 fusion.40
  160.9 0.7 fusion.41
  161.6 0.3 copy-done
  162.0 0.9 fusion.42
  162.9 0.6 dynamic_slice.19
  164.1 1.0 fusion.40
  165.1 0.7 fusion.41
  165.8 0.3 copy-done
  166.1 0.9 fusion.42
  167.1 8.1 %copy.32 = bf16[1,2048,1,128]{3,2,0,1:T(2,128)(2,1)S(1)} copy(bf16[1,2048,1,128]{3,1,2,0:T(8,128)(2,1)S(1)} %bitcast.84) | data formatting | bytes 1048576 | tf_op jit(solution)/shard_map/broadcast_in_dim;reshape | solution.py:98
  175.2 0.5 broadcast.105
  175.7 11.5 %reduce.5 = bf16[2048,128]{1,0:T(8,128)(2,1)S(1)} reduce(bf16[2048,1,1,128]{3,2,1,0:T(2,128)(2,1)S(1)} %bitcast.78, bf16[]{:T(256)} %broadcast.105), dimensions={1,2}, to_apply=%bitcast.65.reduce_sub_computation | reduce | bytes 1048578
  187.3 0.1 reshape.234
  187.4 27.7 %all_to_all.36 = bf16[16,2,8192]{2,1,0:T(2,128)(2,1)S(1)} all-to-all(bf16[16,2,8192]{2,1,0:T(2,128)(2,1)S(1)} %reshape.234), channel_id=1, replica_groups=mesh['grp'=2,'sp'=16,'dp'=16] {'sp'}, dimensions={0} | all-to-all | bytes 1048576 | tf_op jit(solution)/shard_map/all_to_all | solution.py:98
  215.1 0.5 reshape.235
  215.6 0.1 copy.30
  215.7 0.3 copy.29
  216.0 5.5 %fusion.13 = bf16[1,128,2048]{2,1,0:T(8,128)(2,1)} fusion(bf16[128,2048]{0,1:T(8,128)(2,1)S(1)} %bitcast.76, bf16[2048,2048]{1,0:T(8,128)(2,1)} %all-gather.5.cloned.1.call-done), kind=kOutput, calls=%fused_computation.19 | convolution fusion | flops 1074003968 | bytes 9437184 | tf_op jit(solution)/shard_map/dot_general | solution.py:100
  (23 shorter events, 0.3 us)
Async XLA Ops:
  6.5 98.4 %copy-start.1 = (bf16[32,256]{1,0:T(8,128)(2,1)S(1)}, bf16[32,256]{1,0:T(8,128)(2,1)}, u32[]{:S(2)}) copy-start(bf16[32,256]{1,0:T(8,128)(2,1)} %param.12) | copy-start | bytes 49156
  6.5 140.1 %all-gather.3.cloned.1.call-start = ((), (), s32[]{:S(2)}) async-start(), calls=%async_computation.3 | async-start | bytes 2228224 | tf_op jit(solution)/shard_map/all_gather | solution.py:89
  9.3 206.7 %all-gather.5.cloned.1.call-start = ((), (), s32[]{:S(2)}) async-start(), calls=%async_computation.4 | async-start | bytes 8912896 | tf_op jit(solution)/shard_map/all_gather | solution.py:102
  105.7 41.0 %all-to-all-start.1 = ((bf16[16,32,256]{2,1,0:T(8,128)(2,1)}), bf16[16,32,256]{2,1,0:T(8,128)(2,1)S(1)}, u32[]{:S(2)}, u32[]{:S(2)}) async-start(bf16[16,32,256]{2,1,0:T(8,128)(2,1)} %broadcast_in_dim.13), calls=%async_computation.1 | async-start | bytes 524288 | tf_op jit(solution)/shard_map/all_to_all | solution.py:12
  152.5 1.2 copy-start
  156.8 1.0 copy-start
  160.9 1.1 copy-start
  165.1 1.0 copy-start
Sparse Core Ops, SparseCore 0:
  9.4 127.1 all-gather.2
  138.7 67.0 all-gather.4
where the time goes:
time: 229 us; the launch traced here: 228 us
  blocking collectives  152 us (66%)
  local copies, waits for them, and re-layouts  18.1 us (8%)
  other arithmetic  18.1 us (8%)
  matrix products  15.7 us (7%)
  between operations  13.6 us (6%)
  starting transfers between devices  7.86 us (3%)
  loops' own time  2.5 us (1%)
    all_to_all x1, blocking collectives, body(): lax.all_to_all(query_rot[None], 'sp', split_axis=2, concat_axis=1, tiled=...  91.7 us
    all_gather x1, blocking collectives, body(): lax.all_gather(key_rot[None], 'sp', axis=1, tiled=True)  32.2 us
    all_to_all x1, blocking collectives, body(): lax.all_to_all(attended[None], 'sp', split_axis=1, concat_axis=2, tiled=T...  27.7 us
    unnamed x1, other arithmetic  11.5 us
    another operation x1, local copies, waits for them, and re-layouts, body(): attended[None]  8.14 us
    all_to_all x1, starting transfers between devices, sent_to_all(): lax.all_to_all(jnp.broadcast_to(value[None], (length, *value.shape)), axi...  7.79 us
    dot_general x1, matrix products, body(): jnp.dot(flat_rows, lax.all_gather(out_weight, 'dp', axis=1, tiled=True),...  5.46 us
  transfers between devices with their start and end apart: 3, of which 0 were waited for; matrix products, arithmetic and copies ran while one was open for 19% of the time, Pallas kernels for 0%

commit v1 on v0

v1 whole, which is shorter than its diff:
```python
import functools
import math

import jax
import jax.numpy as jnp
import numpy as np
from jax import lax
from jax.experimental import pallas as pl
from jax.experimental.pallas import tpu as pltpu
from jax.sharding import PartitionSpec as P

NOPE = 128
VD = 128
MESH = pl.DeviceIdType.MESH
F32 = jnp.float32
BF16 = jnp.bfloat16
FWD, BWD = 0, 1
LCH = 4
OCH = 8
XPRE = 16
NEG = -1e30


def when(cond, fn):
    if isinstance(cond, (bool, np.bool_)):
        if cond:
            fn()
    else:
        pl.when(cond)(fn)


def kernel(
    nz, ndp,
    q_hbm, lat_hbm, rope_hbm, gain_hbm, wkv_hbm, wout_hbm, cos_hbm, sin_hbm,
    out_hbm,
    lbuf, rbuf, wkv, wout, qraw, qbuf, kbuf, vbuf, sbuf, att, obuf,
    lat, rope, gain, cosv, sinv,
    load_sem, zl_recv, zw_recv, x_recv, xw_recv, dw_recv, do_recv,
    zl_send, zl8_send, zr_send, zw_send, zw8_send, x_send, x4_send, xw_send, dw_send, do_send,
    out_sem,
):
    nx = ndp // 2
    hz, hx = nz // 2, nx // 2
    tok = lat.shape[0]
    kl = lat.shape[1]
    z = lax.axis_index("sp")
    dp = lax.axis_index("dp")
    x = dp // 2
    c = dp % 2
    o = 1 - c
    zdev = [{"sp": (z + 1) % nz}, {"sp": (z + nz - 1) % nz}]
    xdev = [{"dp": (dp + 2) % ndp}, {"dp": (dp + ndp - 2) % ndp}]
    mate = {"dp": x * 2 + o}

    def zsrc(d, s):
        return (z + nz - s) % nz if d == FWD else (z + s) % nz

    def xsrc(d, s):
        return (x + nx - s) % nx if d == FWD else (x + s) % nx

    loads = [
        pltpu.make_async_copy(lat_hbm.at[0], lat, load_sem.at[0]),
        pltpu.make_async_copy(gain_hbm, gain, load_sem.at[1]),
        pltpu.make_async_copy(rope_hbm.at[0], rope, load_sem.at[2]),
        pltpu.make_async_copy(cos_hbm.at[z], cosv, load_sem.at[3]),
        pltpu.make_async_copy(sin_hbm.at[z], sinv, load_sem.at[4]),
        pltpu.make_async_copy(wkv_hbm, wkv.at[z, x, c], load_sem.at[5]),
        pltpu.make_async_copy(wout_hbm, wout.at[c, x], load_sem.at[6]),
        pltpu.make_async_copy(q_hbm.at[0], qraw, load_sem.at[7]),
    ]
    for copy in loads:
        copy.start()

    barrier = pltpu.get_barrier_semaphore()
    peers = zdev + [mate] + [{"dp": (dp + 2 * k) % ndp} for k in range(1, nx)]
    for peer in peers:
        pl.semaphore_signal(barrier, inc=1, device_id=peer, device_id_type=MESH)

    for copy in loads[:5]:
        copy.wait()
    value = lat[...].astype(F32)
    norm = value * lax.rsqrt(jnp.mean(value * value, axis=-1, keepdims=True) + 1e-06)
    lbuf[z] = (norm * gain[...]).astype(BF16)
    half = rope.shape[0] // 2

    def rotated(first, second):
        first = first.astype(F32)
        second = second.astype(F32)
        cosine, sine = cosv[...], sinv[...]
        return first * cosine - second * sine, first * sine + second * cosine

    turned = rotated(rope[0:half, :], rope[half:, :])
    rbuf[z, 0:half, :] = turned[0].astype(BF16)
    rbuf[z, half:, :] = turned[1].astype(BF16)
    loads[5].wait()
    loads[6].wait()
    pl.semaphore_wait(barrier, len(peers))

    rows = tok // LCH
    xs = nx // LCH
    orow = wout.shape[2] // OCH

    def l_ref(b, ch):
        return rbuf.at[b] if ch == LCH else lbuf.at[b, pl.ds(ch * rows, rows)]

    def l_copy(d, s, ch, b):
        if ch == LCH:
            ssem = zr_send.at[d]
        else:
            ssem = zl_send.at[d] if s < hz else zl8_send.at[d]
        return pltpu.make_async_remote_copy(
            src_ref=l_ref(b, ch), dst_ref=l_ref(b, ch), send_sem=ssem,
            recv_sem=zl_recv.at[d, s - 1, ch], device_id=zdev[d], device_id_type=MESH)

    def l_has(d, s, ch):
        if s < hz:
            return True
        return (ch == LCH or ch < LCH // 2) if d == FWD else LCH // 2 <= ch < LCH

    def l_event(s, ch):
        for d in (FWD, BWD):
            if not l_has(d, s, ch):
                continue
            l_copy(d, s, ch, zsrc(d, s)).wait_recv()
            if s < hz and l_has(d, s + 1, ch):
                l_copy(d, s + 1, ch, zsrc(d, s)).start()

    def w_ref(h, ch, core):
        return wkv.at[h, pl.ds(ch * xs, xs), core]

    def w_copy(d, s, ch, h, last):
        return pltpu.make_async_remote_copy(
            src_ref=w_ref(h, ch, c), dst_ref=w_ref(h, ch, c),
            send_sem=zw8_send.at[d] if last else zw_send.at[d],
            recv_sem=zw_recv.at[d, s - 1, ch], device_id=zdev[d], device_id_type=MESH)

    def w_mate(h, ch):
        return pltpu.make_async_remote_copy(
            src_ref=w_ref(h, ch, c), dst_ref=w_ref(h, ch, c), send_sem=dw_send,
            recv_sem=dw_recv.at[h], device_id=mate, device_id_type=MESH)

    def w_event(e):
        s = e // 2 + 1
        part = e % 2
        for d in (FWD, BWD):
            mine = part == d
            h = zsrc(d, s)

            def arrive(d=d, s=s, h=h, part=part):
                for k in range(LCH // 2):
                    w_copy(d, s, part * (LCH // 2) + k, h, False).wait_recv()

            def forward(last, d=d, s=s, h=h, part=part):
                for k in range(LCH // 2):
                    w_copy(d, s + 1, part * (LCH // 2) + k, h, last).start()

            def across(h=h, part=part):
                for k in range(LCH // 2):
                    w_mate(h, part * (LCH // 2) + k).start()

            if isinstance(e, int):
                if s < hz or (s == hz and mine):
                    arrive()
                    if s < hz - 1:
                        forward(False)
                    elif s == hz - 1 and mine:
                        forward(True)
                    across()
            else:
                def body(arrive=arrive, forward=forward, across=across, s=s, mine=mine):
                    arrive()
                    pl.when(s < hz - 1)(lambda: forward(False))
                    pl.when((s == hz - 1) & mine)(lambda: forward(True))
                    across()

                pl.when((s < hz) | ((s == hz) & mine))(body)

    def o_ref(b, ch):
        return wout.at[c, b, pl.ds(ch * orow, orow)]

    def o_copy(d, s, ch, b, last):
        return pltpu.make_async_remote_copy(
            src_ref=o_ref(b, ch), dst_ref=o_ref(b, ch),
            send_sem=x4_send.at[d] if last else x_send.at[d],
            recv_sem=x_recv.at[d, s - 1, ch], device_id=xdev[d], device_id_type=MESH)

    def o_mate(b, ch):
        return pltpu.make_async_remote_copy(
            src_ref=o_ref(b, ch), dst_ref=o_ref(b, ch), send_sem=do_send,
            recv_sem=do_recv, device_id=mate, device_id_type=MESH)

    nev = OCH * (hx - 1) + OCH // 2

    def o_event(n):
        s = n // OCH + 1
        k = n % OCH
        for d in (FWD, BWD):
            b = xsrc(d, s)
            if isinstance(n, int):
                ch = k if s < hx else k + d * (OCH // 2)
                o_copy(d, s, ch, b, False).wait_recv()
                if s < hx - 1:
                    o_copy(d, s + 1, ch, b, False).start()
                elif s == hx - 1 and (k < OCH // 2) == (d == FWD):
                    o_copy(d, s + 1, ch, b, True).start()
                o_mate(b, ch).start()
            else:
                ch = jnp.where(s < hx, k, k + d * (OCH // 2))
                o_copy(d, s, ch, b, False).wait_recv()
                half_ok = (k < OCH // 2) if d == FWD else (k >= OCH // 2)

                def forward(d=d, s=s, ch=ch, b=b, last=False):
                    o_copy(d, s + 1, ch, b, last).start()

                pl.when(s < hx - 1)(forward)
                pl.when((s == hx - 1) & half_ok)(functools.partial(forward, last=True))
                o_mate(b, ch).start()

    def xw_copy(k, b):
        return pltpu.make_async_remote_copy(
            src_ref=wkv.at[z, b, c], dst_ref=wkv.at[z, b, c], send_sem=xw_send,
            recv_sem=xw_recv, device_id={"dp": (dp + 2 * k) % ndp}, device_id_type=MESH)

    for k in range(1, nx):
        xw_copy(k, x).start()
    for ch in range(LCH + 1):
        for d in (FWD, BWD):
            l_copy(d, 1, ch, z).start()
    for ch in range(OCH):
        for d in (FWD, BWD):
            o_copy(d, 1, ch, x, False).start()
    for ch in range(OCH):
        o_mate(x, ch).start()

    def all_of(ref, send_sem, recv_sem):
        return pltpu.make_async_remote_copy(
            src_ref=ref, dst_ref=ref, send_sem=send_sem, recv_sem=recv_sem,
            device_id=mate, device_id_type=MESH)

    loads[7].wait()

    def prepare_query(h):
        content = qraw[h, 0:NOPE, :].astype(F32)
        t0, t1 = rotated(qraw[h, NOPE:NOPE + half, :], qraw[h, NOPE + half:, :])
        pad = jnp.zeros((256 - NOPE - 2 * half, tok), F32)
        whole = jnp.concatenate([content, t0, t1, pad], axis=0)
        qbuf[h] = whole.T.astype(BF16)

    def prepare_key(b):
        key = rbuf[b].astype(F32)
        pad = jnp.zeros((128 - 2 * half, tok), F32)
        kbuf[b, :, NOPE:] = jnp.concatenate([key, pad], axis=0).T.astype(BF16)

    prepare_key(z)
    per = nz // hz
    done = 0
    for s in range(1, hz + 1):
        for ch in range(LCH + 1):
            l_event(s, ch)
            if ch % 2 == 1 and done < XPRE and s > 1:
                o_event(done)
                done += 1
        if s < hz:
            for d in (FWD, BWD):
                prepare_key(zsrc(d, s))
        else:
            prepare_key(zsrc(FWD, s))
        for j in range(per):
            prepare_query((s - 1) * per + j)
        if s == 4:
            all_of(wkv.at[z, pl.ds(0, nx - 1), c], xw_send, xw_recv).wait_recv()
            for ch in range(LCH):
                for d in (FWD, BWD):
                    w_copy(d, 1, ch, z, False).start()
            for ch in range(LCH):
                w_mate(z, ch).start()
    while done < XPRE:
        o_event(done)
        done += 1

    w_event(0)

    span = 4 * tok
    scale = float((2 * half + NOPE) ** -0.5 * math.log2(math.e))

    def one_head(i, carry):
        step = (i + 1) // 2
        h = lax.rem(jnp.where(i % 2 == 1, z + nz - step, z + step), nz)
        all_of(wkv.at[h, :, o], dw_send, dw_recv.at[h]).wait_recv()
        weights = wkv[h].reshape(kl, NOPE + VD)
        for t in range(nz // 4):
            block = lbuf[4 * t:4 * t + 4].reshape(span, kl)
            kv = jnp.dot(block, weights, preferred_element_type=F32).astype(BF16)
            kbuf[4 * t:4 * t + 4, :, 0:NOPE] = kv[:, :NOPE].reshape(4, tok, NOPE)
            vbuf[4 * t:4 * t + 4] = kv[:, NOPE:].reshape(4, tok, VD)
        w_event(i + 1)
        pl.when(i < nev - XPRE)(lambda: o_event(i + XPRE))
        query = qbuf[h]
        row = z * tok + lax.broadcasted_iota(jnp.int32, (tok, span), 0)
        col = lax.broadcasted_iota(jnp.int32, (tok, span), 1)
        top = jnp.full((tok, 128), NEG, F32)
        for t in range(nz // 4):
            keys = kbuf[4 * t:4 * t + 4].reshape(span, 256)
            sc = lax.dot_general(query, keys, (((1,), (1,)), ((), ())), preferred_element_type=F32)
            sc = jnp.where(col + t * span <= row, sc * scale, NEG)
            sbuf[:, t * span:(t + 1) * span] = sc
            for j in range(span // 128):
                top = jnp.maximum(top, sc[:, j * 128:(j + 1) * 128])
        peak = jnp.max(top, axis=-1, keepdims=True)
        total = jnp.zeros((tok, 128), F32)
        result = jnp.zeros((tok, VD), F32)
        for t in range(nz // 4):
            expo = jnp.exp2(sbuf[:, t * span:(t + 1) * span] - peak)
            for j in range(span // 128):
                total = total + expo[:, j * 128:(j + 1) * 128]
            vals = vbuf[4 * t:4 * t + 4].reshape(span, VD)
            result = result + jnp.dot(expo.astype(BF16), vals, preferred_element_type=F32)
        denom = jnp.sum(total, axis=-1, keepdims=True)
        att[h] = (result / denom).astype(BF16)
        return carry

    lax.fori_loop(0, nz, one_head, 0)

    all_of(wout.at[o], do_send, do_recv).wait_recv()
    attended = jnp.concatenate([att[h] for h in range(nz)], axis=1)

    def out_copy(b):
        return pltpu.make_async_copy(
            obuf.at[b], out_hbm.at[0, :, pl.ds(b * 256, 256)], out_sem.at[b])

    def project(b, carry):
        cols = jnp.concatenate([wout[0, b], wout[1, b]], axis=1)
        obuf[b] = jnp.dot(attended, cols, preferred_element_type=F32).astype(BF16)
        out_copy(b).start()
        return carry

    lax.fori_loop(0, nx, project, 0)

    all_of(wkv.at[0, pl.ds(0, nx - 1), 0], xw_send, xw_recv).wait_send()
    for d in (FWD, BWD):
        all_of(lbuf.at[pl.ds(0, hz - 1)], zl_send.at[d], xw_recv).wait_send()
        all_of(lbuf.at[0, pl.ds(0, tok // 2)], zl8_send.at[d], xw_recv).wait_send()
        all_of(rbuf.at[pl.ds(0, hz if d == FWD else hz - 1)], zr_send.at[d], xw_recv).wait_send()
        all_of(wkv.at[pl.ds(0, hz - 1), :, 0], zw_send.at[d], xw_recv).wait_send()
        all_of(wkv.at[0, pl.ds(0, nx // 2), 0], zw8_send.at[d], xw_recv).wait_send()
        all_of(wout.at[0, pl.ds(0, hx - 1)], x_send.at[d], xw_recv).wait_send()
        all_of(wout.at[0, 0, pl.ds(0, wout.shape[2] // 2)], x4_send.at[d], xw_recv).wait_send()
    all_of(wkv.at[:, :, 0], dw_send, xw_recv).wait_send()
    all_of(wout.at[0], do_send, xw_recv).wait_send()
    for b in range(nx):
        out_copy(b).wait()


def body(nz, ndp, queries, kv_latent, rope_key, kv_gain, kv_weight, out_weight):
    tok, heads, width = queries.shape[1:]
    kl = kv_latent.shape[2]
    rot = rope_key.shape[2]
    half = rot // 2
    nx = ndp // 2
    hz, hx = nz // 2, nx // 2
    model = out_weight.shape[1] * ndp
    pos = np.arange(nz * tok, dtype=np.float32)
    inverse = np.power(np.float32(10000.0), -np.arange(half, dtype=np.float32) * np.float32(2.0) / np.float32(rot))
    angle = (pos[:, None] * inverse.astype(np.float32)).astype(np.float32).astype(np.float64)
    table = lambda f: jnp.asarray(
        f(angle).astype(np.float32).reshape(nz, tok, half).transpose(0, 2, 1))
    dma = pltpu.SemaphoreType.DMA
    anyspec = pl.BlockSpec(memory_space=pl.ANY)
    call = pl.pallas_call(
        functools.partial(kernel, nz, ndp),
        out_shape=jax.ShapeDtypeStruct((1, tok, model), BF16),
        in_specs=[anyspec] * 8,
        out_specs=anyspec,
        scratch_shapes=[
            pltpu.VMEM((nz, tok, kl), BF16),
            pltpu.VMEM((nz, rot, tok), BF16),
            pltpu.VMEM((nz, nx, 2, kl // ndp, NOPE + VD), BF16),
            pltpu.VMEM((2, nx, heads * VD, model // ndp), BF16),
            pltpu.VMEM((heads, width, tok), BF16),
            pltpu.VMEM((heads, tok, 256), BF16),
            pltpu.VMEM((nz, tok, 256), BF16),
            pltpu.VMEM((nz, tok, VD), BF16),
            pltpu.VMEM((tok, nz * tok), F32),
            pltpu.VMEM((heads, tok, VD), BF16),
            pltpu.VMEM((nx, tok, 256), BF16),
            pltpu.VMEM((tok, kl), BF16),
            pltpu.VMEM((rot, tok), BF16),
            pltpu.VMEM((1, kl), F32),
            pltpu.VMEM((half, tok), F32),
            pltpu.VMEM((half, tok), F32),
            dma((8,)),
            dma((2, hz, LCH + 1)),
            dma((2, hz, LCH)),
            dma((2, hx, OCH)),
            dma, dma((nz,)), dma,
            dma((2,)), dma((2,)), dma((2,)), dma((2,)), dma((2,)), dma((2,)), dma((2,)),
            dma, dma, dma,
            dma((nx,)),
        ],
        compiler_params=pltpu.CompilerParams(
            collective_id=0, has_side_effects=True, vmem_limit_bytes=60 * 1024 * 1024),
    )
    return call(
        jnp.transpose(queries, (0, 2, 3, 1)), kv_latent, jnp.transpose(rope_key, (0, 2, 1)),
        kv_gain.reshape(1, kl), kv_weight, out_weight, table(np.cos), table(np.sin))


def solution(mesh):
    return jax.shard_map(
        functools.partial(body, mesh.shape["sp"], mesh.shape["dp"]),
        mesh=mesh,
        in_specs=(
            P(("grp", "dp"), "sp", None, None),
            P(("grp", "dp"), "sp", None),
            P(("grp", "dp"), "sp", None),
            P(),
            P("dp", "sp"),
            P(None, "dp"),
        ),
        out_specs=P(("grp", "dp"), "sp", None),
        check_vma=False,
    )
```

time: 229 us -> 121 us (0.53)
  the two profiles are of different devices: /device:TPU:84 before, /device:TPU:65 now
where the time goes in v1:
time: 121 us; the launch traced here: 120 us
  Pallas kernels  119 us (98%)
  local copies, waits for them, and re-layouts  1.88 us (2%)
    pallas_call x1, Pallas kernels, body(): call(jnp.transpose(queries, (0, 2, 3, 1)), kv_latent, jnp.transpose(rope_...  119 us

profile of v1, /device:TPU:65, one launch (start us, length us, event | category | flops | bytes accessed | tf_op | source)
XLA Modules:
  0.0 120.4 jit_solution(17861845975916539)
XLA Ops:
  0.0 118.5 %shard_map.82 = bf16[1,128,2048]{2,1,0:T(8,128)(2,1)} custom-call(bf16[1,16,192,128]{3,2,1,0:T(8,128)(2,1)} %bitcast.3, bf16[1,128,512]{2,1,0:T(8,128)(2,1)} %lat_hbm.1, bf16[1,64,128]{2,1,0:T(8,128)(2,1)} %bitcast.4, f32[1,512]{1,0:T(1,128)} %bitcast.5, bf16[32,256]{1,0:T(8,128)(2,1)} %wkv_hbm.1, bf16[2048,128]{1,0:T(8,128)(2,1)} %wout_hbm.1, ...), custom_call_target="tpu_custom_call" | custom-call | tf_op jit(solution)/shard_map/pallas_call | solution.py:403
  118.5 1.9 %copy.10 = bf16[1,128,2048]{2,1,0:T(8,128)(2,1)} copy(bf16[1,128,2048]{2,1,0:T(8,128)(2,1)} %shard_map.82) | data formatting | bytes 1048576

commit v2 on v1

v2 whole, which is shorter than its diff:
```python
import functools
import math

import jax
import jax.numpy as jnp
import numpy as np
from jax import lax
from jax.experimental import pallas as pl
from jax.experimental.pallas import tpu as pltpu
from jax.sharding import PartitionSpec as P

NOPE = 128
VD = 128
MESH = pl.DeviceIdType.MESH
F32 = jnp.float32
BF16 = jnp.bfloat16
FWD, BWD = 0, 1
LCH = 4
OCH = 8
WSTART = 6
WPRE = 5
XPRE = 16
NEG = -1e30


def kernel(
    nz, ndp,
    q_hbm, lat_hbm, rope_hbm, gain_hbm, wkv_hbm, wout_hbm, cos_hbm, sin_hbm,
    out_hbm,
    lbuf, rbuf, wkv, wout, qraw, qbuf, krot, kbuf, vbuf, sbuf, peak, att, obuf,
    lat, rope, gain, cosv, sinv,
    load_sem, zl_recv, zw_recv, x_recv, xw_recv, dw_recv, do_recv,
    zl_send, zd_send, zw_send, zw8_send, x_send, x4_send, xw_send, dw_send, do_send,
    out_sem, up_ready, wrap_ready, first_in,
):
    nx = ndp // 2
    hz, hx = nz // 2, nx // 2
    tok = lat.shape[0]
    kl = lat.shape[1]
    z = lax.axis_index("sp")
    dp = lax.axis_index("dp")
    x = dp // 2
    c = dp % 2
    o = 1 - c
    zdev = [{"sp": (z + 1) % nz}, {"sp": (z + nz - 1) % nz}]
    xdev = [{"dp": (dp + 2) % ndp}, {"dp": (dp + ndp - 2) % ndp}]
    mate = {"dp": x * 2 + o}

    def xsrc(d, s):
        return (x + nx - s) % nx if d == FWD else (x + s) % nx

    loads = [
        pltpu.make_async_copy(lat_hbm.at[0], lat, load_sem.at[0]),
        pltpu.make_async_copy(gain_hbm, gain, load_sem.at[1]),
        pltpu.make_async_copy(rope_hbm.at[0], rope, load_sem.at[2]),
        pltpu.make_async_copy(cos_hbm.at[z], cosv, load_sem.at[3]),
        pltpu.make_async_copy(sin_hbm.at[z], sinv, load_sem.at[4]),
        pltpu.make_async_copy(wkv_hbm, wkv.at[z, x, c], load_sem.at[5]),
        pltpu.make_async_copy(wout_hbm, wout.at[c, x], load_sem.at[6]),
        pltpu.make_async_copy(q_hbm.at[0], qraw, load_sem.at[7]),
    ]
    for copy in loads:
        copy.start()

    def clear(b, carry):
        lbuf[b] = jnp.zeros(lbuf.shape[1:], BF16)
        krot[b] = jnp.zeros(krot.shape[1:], BF16)
        return carry

    lax.fori_loop(1, nz, clear, 0)

    barrier = pltpu.get_barrier_semaphore()

    def tell(sem, peer):
        pl.semaphore_signal(sem, inc=1, device_id=peer, device_id_type=MESH)

    for peer in [mate] + [{"dp": (dp + 2 * k) % ndp} for k in range(1, nx)]:
        tell(barrier, peer)
    pl.when(z < nz - 1)(lambda: tell(barrier, zdev[FWD]))
    pl.when(z == 0)(lambda: tell(barrier, zdev[BWD]))

    for copy in loads[:5]:
        copy.wait()
    value = lat[...].astype(F32)
    norm = value * lax.rsqrt(jnp.mean(value * value, axis=-1, keepdims=True) + 1e-06)
    lbuf[0] = (norm * gain[...]).astype(BF16)
    half = rope.shape[0] // 2

    def rotated(first, second):
        first = first.astype(F32)
        second = second.astype(F32)
        cosine, sine = cosv[...], sinv[...]
        return first * cosine - second * sine, first * sine + second * cosine

    turned = rotated(rope[0:half, :], rope[half:, :])
    rbuf[0, 0:half, :] = turned[0].astype(BF16)
    rbuf[0, half:, :] = turned[1].astype(BF16)
    loads[5].wait()
    loads[6].wait()
    pl.semaphore_wait(barrier, nx + jnp.where(z > 0, 1, 0) + jnp.where(z == nz - 1, 1, 0))
    pl.when(z > 0)(lambda: tell(up_ready, zdev[BWD]))
    pl.when(z == nz - 1)(lambda: tell(wrap_ready, zdev[FWD]))

    rows = tok // LCH
    xs = nx // LCH
    orow = wout.shape[2] // OCH

    def slot(d, s):
        return s if d == FWD else (nz - s) % nz

    def all_of(ref, send_sem, recv_sem):
        return pltpu.make_async_remote_copy(
            src_ref=ref, dst_ref=ref, send_sem=send_sem, recv_sem=recv_sem,
            device_id=mate, device_id_type=MESH)

    def l_ref(b, ch):
        return rbuf.at[b] if ch == LCH else lbuf.at[b, pl.ds(ch * rows, rows)]

    def l_copy(d, s, ch):
        return pltpu.make_async_remote_copy(
            src_ref=l_ref(slot(d, s - 1), ch), dst_ref=l_ref(slot(d, s), ch),
            send_sem=zl_send.at[d, s - 1, ch], recv_sem=zl_recv.at[d, s - 1, ch],
            device_id=zdev[d], device_id_type=MESH)

    def furthest(d, ch):
        low = ch == LCH or ch < LCH // 2
        return hz if low == (d == FWD) else hz - 1

    def l_got(d, s, ch):
        if d == FWD:
            return z >= s
        return (z + s >= nz) | (z + s <= furthest(d, ch) - 1)

    def l_sent(d, s, ch):
        if d == FWD:
            return (z < nz - 1) & (z >= s - 1)
        return (z == 0) | (z + s - 1 >= nz) | (z + s - 1 <= furthest(d, ch) - 1)

    def l_event(s, ch):
        for d in (FWD, BWD):
            if s > furthest(d, ch):
                continue

            def body(d=d):
                l_copy(d, s, ch).wait_recv()
                if s + 1 <= furthest(d, ch):
                    pl.when(z < nz - 1 if d == FWD else z > 0)(l_copy(d, s + 1, ch).start)

            pl.when(l_got(d, s, ch))(body)

    def w_ref(h, ch, core):
        return wkv.at[h, pl.ds(ch * xs, xs), core]

    def w_copy(d, s, ch, h, ssem, device=None):
        return pltpu.make_async_remote_copy(
            src_ref=w_ref(h, ch, c), dst_ref=w_ref(h, ch, c), send_sem=ssem,
            recv_sem=zw_recv.at[d, s - 1, ch], device_id=zdev[d] if device is None else device,
            device_id_type=MESH)

    def w_mate(h, ch):
        return pltpu.make_async_remote_copy(
            src_ref=w_ref(h, ch, c), dst_ref=w_ref(h, ch, c), send_sem=dw_send,
            recv_sem=dw_recv.at[h], device_id=mate, device_id_type=MESH)

    nwe = LCH * (hz - 1) + LCH // 2

    def forward_distance(k):
        return jnp.where(k < z, k + 1, hz - 1 - (k - z))

    def w_event(n):
        n = jnp.int32(n)
        k = n // LCH
        j = n % LCH
        final = k == hz - 1
        for d in (FWD, BWD):
            s = jnp.where(final, hz, forward_distance(k)) if d == FWD else k + 1
            h = lax.rem(z + nz - s if d == FWD else z + s, nz)
            ch = j if d == FWD else jnp.where(final, j + LCH // 2, j)
            half_ok = (j < LCH // 2) if d == FWD else (j >= LCH // 2)
            may = z < nz - 1 if d == FWD else z >= 0
            w_copy(d, s, ch, h, zw_send.at[d]).wait_recv()
            pl.when(may & (s < hz - 1))(w_copy(d, s + 1, ch, h, zw_send.at[d]).start)
            pl.when(may & (s == hz - 1) & half_ok)(w_copy(d, s + 1, ch, h, zw8_send.at[d]).start)
            w_mate(h, ch).start()

    def o_ref(b, ch):
        return wout.at[c, b, pl.ds(ch * orow, orow)]

    def o_copy(d, s, ch, b, last):
        return pltpu.make_async_remote_copy(
            src_ref=o_ref(b, ch), dst_ref=o_ref(b, ch),
            send_sem=x4_send.at[d] if last else x_send.at[d],
            recv_sem=x_recv.at[d, s - 1, ch], device_id=xdev[d], device_id_type=MESH)

    def o_mate(b, ch):
        return pltpu.make_async_remote_copy(
            src_ref=o_ref(b, ch), dst_ref=o_ref(b, ch), send_sem=do_send,
            recv_sem=do_recv, device_id=mate, device_id_type=MESH)

    nev = OCH * (hx - 1) + OCH // 2

    def o_event(n):
        s = n // OCH + 1
        k = n % OCH
        for d in (FWD, BWD):
            b = xsrc(d, s)
            if isinstance(n, int):
                ch = k if s < hx else k + d * (OCH // 2)
                o_copy(d, s, ch, b, False).wait_recv()
                if s < hx - 1:
                    o_copy(d, s + 1, ch, b, False).start()
                elif s == hx - 1 and (k < OCH // 2) == (d == FWD):
                    o_copy(d, s + 1, ch, b, True).start()
                o_mate(b, ch).start()
            else:
                ch = jnp.where(s < hx, k, k + d * (OCH // 2))
                o_copy(d, s, ch, b, False).wait_recv()
                half_ok = (k < OCH // 2) if d == FWD else (k >= OCH // 2)

                def forward(d=d, s=s, ch=ch, b=b, last=False):
                    o_copy(d, s + 1, ch, b, last).start()

                pl.when(s < hx - 1)(forward)
                pl.when((s == hx - 1) & half_ok)(functools.partial(forward, last=True))
                o_mate(b, ch).start()

    for k in range(1, nx):
        pltpu.make_async_remote_copy(
            src_ref=wkv.at[z, x, c], dst_ref=wkv.at[z, x, c], send_sem=xw_send,
            recv_sem=xw_recv, device_id={"dp": (dp + 2 * k) % ndp}, device_id_type=MESH).start()
    for ch in range(LCH + 1):
        pl.when((z > 0) & (z <= furthest(BWD, ch) - 1))(l_copy(BWD, 1, ch).start)
    for ch in range(OCH):
        for d in (FWD, BWD):
            o_copy(d, 1, ch, x, False).start()
    for ch in range(OCH):
        o_mate(x, ch).start()

    def up_first():
        pl.semaphore_wait(up_ready, 1)
        for ch in range(LCH + 1):
            l_copy(FWD, 1, ch).start()

    pl.when(z < nz - 1)(up_first)
    loads[7].wait()

    def prepare_query(h):
        content = qraw[h, 0:NOPE, :].astype(F32)
        t0, t1 = rotated(qraw[h, NOPE:NOPE + half, :], qraw[h, NOPE + half:, :])
        pad = jnp.zeros((256 - NOPE - 2 * half, tok), F32)
        whole = jnp.concatenate([content, t0, t1, pad], axis=0)
        qbuf[h] = whole.T.astype(BF16)

    def prepare_key(b):
        key = rbuf[b].astype(F32)
        pad = jnp.zeros((128 - 2 * half, tok), F32)
        krot[b] = jnp.concatenate([key, pad], axis=0).T.astype(BF16)

    prepare_key(0)
    per = nz // hz
    done = 0
    for s in range(1, hz + 1):
        for ch in range(LCH + 1):
            l_event(s, ch)
            if ch % 2 == 1 and done < XPRE and s > 1:
                o_event(done)
                done += 1
        for d in (FWD, BWD) if s < hz else (FWD,):
            pl.when(z >= slot(d, s))(functools.partial(prepare_key, slot(d, s)))
        for j in range(per):
            prepare_query((s - 1) * per + j)
        if s == 2:
            all_of(wkv.at[z, pl.ds(0, nx - 1), c], xw_send, xw_recv).wait_recv()
            pl.when(z > 1)(lambda: pl.semaphore_wait(first_in, 1))
            pl.when((z > 0) & (z < nz - 1))(lambda: tell(first_in, zdev[FWD]))
            for ch in range(LCH):
                pl.when(z >= hz if ch < LCH // 2 else z > hz)(
                    w_copy(FWD, nz - z, ch, z, zd_send.at[ch], {"sp": 0}).start)
                pl.when(z > 0)(w_copy(BWD, 1, ch, z, zw_send.at[BWD]).start)
                pl.when(z < hz)(w_copy(FWD, 1, ch, z, zw_send.at[FWD]).start)
            for ch in range(LCH):
                w_mate(z, ch).start()
        if s == WSTART:
            for ch in range(LCH):
                pl.when((z >= hz) & (z < nz - 1))(w_copy(FWD, 1, ch, z, zw_send.at[FWD]).start)

    def round_the_wrap():
        pl.semaphore_wait(wrap_ready, 1)
        for s in range(1, hz + 1):
            for ch in range(LCH + 1):
                if s <= furthest(BWD, ch):
                    l_copy(BWD, s, ch).start()
        for ch in range(LCH):
            w_copy(BWD, 1, ch, z, zw_send.at[BWD]).start()

    pl.when(z == 0)(round_the_wrap)
    while done < XPRE:
        o_event(done)
        done += 1

    span = 4 * tok
    parts = nz // 4
    scale = float((2 * half + NOPE) ** -0.5 * math.log2(math.e))

    bias = [None] + [jnp.where(z >= j, 0.0, NEG).astype(F32) for j in range(1, nz)]
    sizes = [(z < 4, 1), ((z >= 4) & (z < 8), 2), (z >= 8, parts)]

    def up_project(h, par, t):
        weights = wkv[h].reshape(kl, NOPE + VD)
        block = lbuf[4 * t:4 * t + 4].reshape(span, kl)
        kv = jnp.dot(block, weights, preferred_element_type=F32).astype(BF16)
        kbuf[par, 4 * t:4 * t + 4] = kv[:, :NOPE].reshape(4, tok, NOPE)
        vbuf[par, 4 * t:4 * t + 4] = kv[:, NOPE:].reshape(4, tok, VD)

    def head_of(i):
        k = i // 2
        ahead = jnp.where(i == nz - 1, hz, jnp.where(i % 2 == 1, nz - forward_distance(k), k))
        return lax.rem(z + ahead, nz)

    def find_scores(h, par, tiles):
        query = qbuf[h]
        top = jnp.full((tok, 128), NEG, F32)
        for t in range(tiles):
            keys = jnp.concatenate(
                [kbuf[par, 4 * t:4 * t + 4].reshape(span, NOPE),
                 krot[4 * t:4 * t + 4].reshape(span, 128)], axis=1)
            sc = lax.dot_general(query, keys, (((1,), (1,)), ((), ())), preferred_element_type=F32)
            for j in range(4):
                piece = sc[:, j * tok:(j + 1) * tok] * scale
                if t == 0 and j == 0:
                    row = lax.broadcasted_iota(jnp.int32, (tok, tok), 0)
                    col = lax.broadcasted_iota(jnp.int32, (tok, tok), 1)
                    piece = jnp.where(col <= row, piece, NEG)
                else:
                    piece = piece + bias[4 * t + j]
                sbuf[:, (4 * t + j) * tok:(4 * t + j + 1) * tok] = piece
                top = jnp.maximum(top, piece)
        peak[...] = jnp.broadcast_to(jnp.max(top, axis=-1, keepdims=True), (tok, 128))

    def attend(h, par, tiles, following):
        high = jnp.max(peak[...], axis=-1, keepdims=True)
        total = jnp.zeros((tok, 128), F32)
        result = jnp.zeros((tok, VD), F32)
        for t in range(tiles):
            expo = jnp.exp2(sbuf[:, t * span:(t + 1) * span] - high)
            for j in range(span // 128):
                total = total + expo[:, j * 128:(j + 1) * 128]
            vals = vbuf[par, 4 * t:4 * t + 4].reshape(span, VD)
            result = result + jnp.dot(expo.astype(BF16), vals, preferred_element_type=F32)
            if following is not None:
                up_project(following, 1 - par, t)
        denom = jnp.sum(total, axis=-1, keepdims=True)
        att[h] = (result / denom).astype(BF16)

    for n in range(WPRE):
        w_event(n)
    all_of(wkv.at[z, :, o], dw_send, dw_recv.at[z]).wait_recv()
    for t in range(parts):
        pl.when(z >= min(4 * t, 8))(functools.partial(up_project, z, 0, t))

    def one_head(i, carry):
        par = lax.rem(i, 2)
        h, following = head_of(i), head_of(i + 1)
        for cond, tiles in sizes:
            pl.when(cond)(functools.partial(find_scores, h, par, tiles))
        pl.when(2 * i + WPRE < nwe)(lambda: w_event(2 * i + WPRE))
        pl.when(i < nev - XPRE)(lambda: o_event(i + XPRE))
        all_of(wkv.at[following, :, o], dw_send, dw_recv.at[following]).wait_recv()
        for cond, tiles in sizes:
            pl.when(cond)(functools.partial(attend, h, par, tiles, following))
        pl.when(2 * i + WPRE + 1 < nwe)(lambda: w_event(2 * i + WPRE + 1))
        return carry

    lax.fori_loop(0, nz - 1, one_head, 0)
    last_head = head_of(jnp.int32(nz - 1))
    for cond, tiles in sizes:
        pl.when(cond)(functools.partial(find_scores, last_head, (nz - 1) % 2, tiles))
        pl.when(cond)(functools.partial(attend, last_head, (nz - 1) % 2, tiles, None))

    all_of(wout.at[o], do_send, do_recv).wait_recv()
    attended = jnp.concatenate([att[h] for h in range(nz)], axis=1)

    def out_copy(b):
        return pltpu.make_async_copy(
            obuf.at[b], out_hbm.at[0, :, pl.ds(b * 256, 256)], out_sem.at[b])

    def project(b, carry):
        cols = jnp.concatenate([wout[0, b], wout[1, b]], axis=1)
        obuf[b] = jnp.dot(attended, cols, preferred_element_type=F32).astype(BF16)
        out_copy(b).start()
        return carry

    lax.fori_loop(0, nx, project, 0)

    all_of(wkv.at[0, pl.ds(0, nx - 1), 0], xw_send, xw_recv).wait_send()
    for s in range(1, hz + 1):
        for ch in range(LCH + 1):
            for d in (FWD, BWD):
                if s <= furthest(d, ch):
                    pl.when(l_sent(d, s, ch))(l_copy(d, s, ch).wait_send)
    for ch in range(LCH):
        pl.when(z >= hz if ch < LCH // 2 else z > hz)(
            w_copy(FWD, 1, ch, z, zd_send.at[ch]).wait_send)
    for d in (FWD, BWD):

        def weights_sent(d=d):
            all_of(wkv.at[pl.ds(0, hz - 1), :, 0], zw_send.at[d], xw_recv).wait_send()
            all_of(wkv.at[0, pl.ds(0, nx // 2), 0], zw8_send.at[d], xw_recv).wait_send()

        pl.when(z < nz - 1 if d == FWD else z >= 0)(weights_sent)
        all_of(wout.at[0, pl.ds(0, hx - 1)], x_send.at[d], xw_recv).wait_send()
        all_of(wout.at[0, 0, pl.ds(0, wout.shape[2] // 2)], x4_send.at[d], xw_recv).wait_send()
    all_of(wkv.at[:, :, 0], dw_send, xw_recv).wait_send()
    all_of(wout.at[0], do_send, xw_recv).wait_send()
    for b in range(nx):
        out_copy(b).wait()


def body(nz, ndp, queries, kv_latent, rope_key, kv_gain, kv_weight, out_weight):
    tok, heads, width = queries.shape[1:]
    kl = kv_latent.shape[2]
    rot = rope_key.shape[2]
    half = rot // 2
    nx = ndp // 2
    hz, hx = nz // 2, nx // 2
    model = out_weight.shape[1] * ndp
    pos = np.arange(nz * tok, dtype=np.float32)
    inverse = np.power(np.float32(10000.0), -np.arange(half, dtype=np.float32) * np.float32(2.0) / np.float32(rot))
    angle = (pos[:, None] * inverse.astype(np.float32)).astype(np.float32).astype(np.float64)
    table = lambda f: jnp.asarray(
        f(angle).astype(np.float32).reshape(nz, tok, half).transpose(0, 2, 1))
    dma = pltpu.SemaphoreType.DMA
    anyspec = pl.BlockSpec(memory_space=pl.ANY)
    call = pl.pallas_call(
        functools.partial(kernel, nz, ndp),
        out_shape=jax.ShapeDtypeStruct((1, tok, model), BF16),
        in_specs=[anyspec] * 8,
        out_specs=anyspec,
        scratch_shapes=[
            pltpu.VMEM((nz, tok, kl), BF16),
            pltpu.VMEM((nz, rot, tok), BF16),
            pltpu.VMEM((nz, nx, 2, kl // ndp, NOPE + VD), BF16),
            pltpu.VMEM((2, nx, heads * VD, model // ndp), BF16),
            pltpu.VMEM((heads, width, tok), BF16),
            pltpu.VMEM((heads, tok, 256), BF16),
            pltpu.VMEM((nz, tok, 128), BF16),
            pltpu.VMEM((2, nz, tok, NOPE), BF16),
            pltpu.VMEM((2, nz, tok, VD), BF16),
            pltpu.VMEM((tok, nz * tok), F32),
            pltpu.VMEM((tok, 128), F32),
            pltpu.VMEM((heads, tok, VD), BF16),
            pltpu.VMEM((nx, tok, 256), BF16),
            pltpu.VMEM((tok, kl), BF16),
            pltpu.VMEM((rot, tok), BF16),
            pltpu.VMEM((1, kl), F32),
            pltpu.VMEM((half, tok), F32),
            pltpu.VMEM((half, tok), F32),
            dma((8,)),
            dma((2, hz, LCH + 1)),
            dma((2, hz, LCH)),
            dma((2, hx, OCH)),
            dma, dma((nz,)), dma,
            dma((2, hz, LCH + 1)), dma((LCH,)), dma((2,)), dma((2,)), dma((2,)), dma((2,)),
            dma, dma, dma,
            dma((nx,)),
            pltpu.SemaphoreType.REGULAR, pltpu.SemaphoreType.REGULAR, pltpu.SemaphoreType.REGULAR,
        ],
        compiler_params=pltpu.CompilerParams(
            collective_id=0, has_side_effects=True, vmem_limit_bytes=60 * 1024 * 1024),
    )
    return call(
        jnp.transpose(queries, (0, 2, 3, 1)), kv_latent, jnp.transpose(rope_key, (0, 2, 1)),
        kv_gain.reshape(1, kl), kv_weight, out_weight, table(np.cos), table(np.sin))


def solution(mesh):
    return jax.shard_map(
        functools.partial(body, mesh.shape["sp"], mesh.shape["dp"]),
        mesh=mesh,
        in_specs=(
            P(("grp", "dp"), "sp", None, None),
            P(("grp", "dp"), "sp", None),
            P(("grp", "dp"), "sp", None),
            P(),
            P("dp", "sp"),
            P(None, "dp"),
        ),
        out_specs=P(("grp", "dp"), "sp", None),
        check_vma=False,
    )
```

time: 121 us -> 131 us (1.083)
  the two profiles are of different devices: /device:TPU:65 before, /device:TPU:448 now
where the time goes in v2:
time: 131 us; the launch traced here: 130 us
  Pallas kernels  129 us (98%)
  local copies, waits for them, and re-layouts  1.88 us (1%)
    pallas_call x1, Pallas kernels, body(): call(jnp.transpose(queries, (0, 2, 3, 1)), kv_latent, jnp.transpose(rope_...  129 us

profile of v2, /device:TPU:448, one launch (start us, length us, event | category | flops | bytes accessed | tf_op | source)
XLA Modules:
  0.0 130.4 jit_solution(5623584745490007769)
XLA Ops:
  0.0 128.5 %shard_map.82 = bf16[1,128,2048]{2,1,0:T(8,128)(2,1)} custom-call(bf16[1,16,192,128]{3,2,1,0:T(8,128)(2,1)} %bitcast.3, bf16[1,128,512]{2,1,0:T(8,128)(2,1)} %lat_hbm.1, bf16[1,64,128]{2,1,0:T(8,128)(2,1)} %bitcast.4, f32[1,512]{1,0:T(1,128)} %bitcast.5, bf16[32,256]{1,0:T(8,128)(2,1)} %wkv_hbm.1, bf16[2048,128]{1,0:T(8,128)(2,1)} %wout_hbm.1, ...), custom_call_target="tpu_custom_call" | custom-call | tf_op jit(solution)/shard_map/pallas_call | solution.py:471
  128.5 1.9 %copy.10 = bf16[1,128,2048]{2,1,0:T(8,128)(2,1)} copy(bf16[1,128,2048]{2,1,0:T(8,128)(2,1)} %shard_map.82) | data formatting | bytes 1048576
